TPU v7x, 32 devices: a whole 2x2x4 slice. The times are simulated.
32 devices in a mesh: rep: 4 (over z), fs: 4 (over y, x), tp: 2 (over core).
Axes of the slice: x: 2, y: 2, z: 4, core: 2. Of those that a mesh axis runs over, the one named last changes fastest.
Arguments:
- inputs: bfloat16 [2048, 2048], P('rep', 'fs'), may hold values from -6 to 6
- w_gate: bfloat16 [2048, 3072], P('fs', 'tp'), may hold values from -0.125 to 0.125
- w_up: bfloat16 [2048, 3072], P('fs', 'tp'), may hold values from -0.125 to 0.125
- conv_taps: bfloat16 [3, 3072], P(None, 'tp'), may hold values from -3.5 to 3.5
- w_down: bfloat16 [3072, 2048], P('tp', 'fs'), may hold values from -0.109375 to 0.109375
- out_grad: bfloat16 [2048, 2048], P('rep', 'fs'), may hold values from -6 to 6
Outputs:
- in_grad: bfloat16 [2048, 2048], P(('rep', 'tp'), 'fs')
- grad_gate: float32 [2048, 3072], P('fs', 'tp')
- grad_up: float32 [2048, 3072], P('fs', 'tp')
- grad_down: float32 [3072, 2048], P('tp', 'fs')
- grad_taps: float32 [3, 3072], P(None, 'tp')
- rows_gate: float32 [2048], P('fs')
- rows_up: float32 [2048], P('fs')
- rows_down: float32 [3072], P('tp')
All inputs are finite; a program needn't handle non-finite values.
Results may differ from a plain program's by a relative error of at most 0.025.
Values may be sent and summed in bfloat16 or wider, within the bound.
A program may use at most 64 MiB of HBM per device.

v0:
```python
import jax
import jax.numpy as jnp
from jax import lax
from jax.sharding import PartitionSpec as P

KW = 3


def shift_down(values, lag_rows):
    if lag_rows == 0:
        return values
    padding = jnp.zeros_like(values[:lag_rows])
    return jnp.concatenate([padding, values[:-lag_rows]], axis=0)


def shift_up(values, lag_rows):
    if lag_rows == 0:
        return values
    padding = jnp.zeros_like(values[:lag_rows])
    return jnp.concatenate([values[lag_rows:], padding], axis=0)


def contract(left, right, left_dim, right_dim):
    return lax.dot_general(
        left, right, (((left_dim,), (right_dim,)), ((), ())), preferred_element_type=jnp.float32
    )


def row_norms(grad_gate, grad_up, grad_down):
    gate_rows = jnp.sum(grad_gate * grad_gate, axis=1)
    up_rows = jnp.sum(grad_up * grad_up, axis=1)
    down_rows = jnp.sum(grad_down * grad_down, axis=1)
    gate_rows, up_rows = lax.psum((gate_rows, up_rows), "tp")
    down_rows = lax.psum(down_rows, "fs")
    return (gate_rows, up_rows, down_rows)


def shards(inputs, w_gate, w_up, conv_taps, w_down, out_grad):
    tap_weights = conv_taps.astype(jnp.float32)
    gate_part = jnp.dot(inputs, w_gate, preferred_element_type=jnp.float32)
    up_part = jnp.dot(inputs, w_up, preferred_element_type=jnp.float32)
    act_part = contract(out_grad, w_down, 1, 1)
    gate_sum, up_sum, act_sum = (
        lax.psum(gate_part.astype(jnp.bfloat16), "fs").astype(jnp.float32),
        lax.psum(up_part.astype(jnp.bfloat16), "fs").astype(jnp.float32),
        lax.psum(act_part.astype(jnp.bfloat16), "fs").astype(jnp.float32),
    )
    gate_pre = gate_sum.astype(jnp.bfloat16)
    up_val = up_sum.astype(jnp.bfloat16)
    act_grad = act_sum.astype(jnp.bfloat16)
    gate_float = gate_pre.astype(jnp.float32)
    up_float = up_val.astype(jnp.float32)
    act_float = act_grad.astype(jnp.float32)
    shifted = [shift_down(gate_float, KW - 1 - tap_index) for tap_index in range(KW)]
    pre_act = tap_weights[0] * shifted[0]
    for tap_index in range(1, KW):
        pre_act = pre_act + tap_weights[tap_index] * shifted[tap_index]
    sigmoid_pre = jax.nn.sigmoid(pre_act)
    hidden = (pre_act * sigmoid_pre * up_float).astype(jnp.bfloat16)
    up_grad = (act_float * pre_act * sigmoid_pre).astype(jnp.bfloat16)
    pre_grad = act_float * up_float * sigmoid_pre * (1.0 + pre_act * (1.0 - sigmoid_pre))
    gate_acc = tap_weights[0] * shift_up(pre_grad, KW - 1)
    for tap_index in range(1, KW):
        gate_acc = gate_acc + tap_weights[tap_index] * shift_up(pre_grad, KW - 1 - tap_index)
    gate_grad = gate_acc.astype(jnp.bfloat16)
    gate_rows = gate_grad
    up_rows = up_grad
    in_grad = lax.psum_scatter(
        (contract(gate_rows, w_gate, 1, 1) + contract(up_rows, w_up, 1, 1)).astype(jnp.bfloat16),
        "tp",
        scatter_dimension=0,
        tiled=True,
    )
    grad_gate = contract(inputs, gate_grad, 0, 0)
    grad_up = contract(inputs, up_grad, 0, 0)
    grad_down = contract(hidden, out_grad, 0, 0)
    grad_taps = jnp.stack(
        [jnp.sum(shifted[tap_index] * pre_grad, axis=0) for tap_index in range(KW)]
    )
    grad_gate, grad_up, grad_down, grad_taps = (
        lax.psum(grad_gate.astype(jnp.bfloat16), "rep").astype(jnp.float32),
        lax.psum(grad_up.astype(jnp.bfloat16), "rep").astype(jnp.float32),
        lax.psum(grad_down.astype(jnp.bfloat16), "rep").astype(jnp.float32),
        lax.psum(grad_taps.astype(jnp.bfloat16), "rep").astype(jnp.float32),
    )
    gate_rows, up_rows, down_rows = row_norms(grad_gate, grad_up, grad_down)
    weight_grads = (grad_gate, grad_up, grad_down, grad_taps, gate_rows, up_rows, down_rows)
    grad_gate, grad_up, grad_down, grad_taps, gate_rows, up_rows, down_rows = weight_grads
    return (in_grad, grad_gate, grad_up, grad_down, grad_taps, gate_rows, up_rows, down_rows)


def solution(mesh):
    return jax.shard_map(
        shards,
        mesh=mesh,
        in_specs=(
            P("rep", "fs"),
            P("fs", "tp"),
            P("fs", "tp"),
            P(None, "tp"),
            P("tp", "fs"),
            P("rep", "fs"),
        ),
        out_specs=(
            P(("rep", "tp"), "fs"),
            P("fs", "tp"),
            P("fs", "tp"),
            P("tp", "fs"),
            P(None, "tp"),
            P("fs"),
            P("fs"),
            P("tp"),
        ),
        check_vma=False,
    )
```

profile of v0, /device:TPU:0, one launch (start us, length us, event | category | flops | bytes accessed | tf_op | source)
XLA Modules:
  0.0 352.9 jit_solution(3021039678439691486)
XLA Ops:
  7.2 0.0 copy-start
  7.2 0.0 copy-start.8
  7.2 0.0 all-reduce.10.cloned.1.call-start
  7.2 1.3 copy-done
  8.6 3.2 convolution_convert_fusion.3
  11.8 0.0 copy-done.8
  11.8 0.0 copy-done.12
  11.8 2.1 convolution_convert_fusion.4
  14.0 0.0 copy-done.7
  14.0 0.0 copy-done.10
  14.0 2.2 convolution_convert_fusion.5
  16.1 0.0 all-reduce.10.cloned.1.call-update
  16.2 0.0 all-reduce.12.cloned.1.call-start
  16.2 0.6 copy-done.6
  16.8 0.1 slice_reduce_fusion.2
  16.9 114.4 %all-reduce.10.cloned.1.call-done = (bf16[512,1536]{1,0:T(8,128)(2,1)}, bf16[512,1536]{1,0:T(8,128)(2,1)}, bf16[512,1536]{1,0:T(8,128)(2,1)}) async-done(((bf16[512,1536]{1,0:T(8,128)(2,1)}, bf16[512,1536]{1,0:T(8,128)(2,1)}, bf16[512,1536]{1,0:T(8,128)(2,1)}), (bf16[512,1536]{1,0:T(8,128)(2,1)}, bf16[512,1536]{1,0:T(8,128)(2,1)}, bf16[512,1536]{1,0:T(8,128)(2,1)})) %all-reduce.10.cloned.1.call-update) | async-done | bytes 4718608 | tf_op jit(solution)/shard_map/psum | solution.py:44
  131.3 1.9 slice.32
  133.3 0.4 slice.34
  133.7 1.0 copy-done.2
  134.7 0.5 copy-done.4
  135.2 3.2 multiply_reduce_fusion.5
  138.3 0.4 slice.36
  138.7 0.0 copy-start.11
  138.7 0.4 slice.37
  139.1 0.7 copy-done.11
  139.7 2.4 convolution_convert_fusion
  142.2 1.9 fusion.1
  144.1 0.0 copy-start.5
  144.1 0.0 copy-done.13
  144.1 2.2 fusion.5
  146.2 0.0 copy-done.5
  146.3 2.2 fusion.6
  148.4 0.0 all-reduce.12.cloned.1.call-update
  148.4 0.0 reduce-scatter.2.cloned.1.call-start
  148.5 0.0 copy-start.9
  148.5 2.5 fusion.11
  151.1 1.8 fusion.8
  152.9 0.0 reduce-scatter.2.cloned.1.call-update
  153.0 20.6 %psum.76 = bf16[3,1536]{1,0:T(4,128)(2,1)S(1)} all-reduce(bf16[3,1536]{1,0:T(4,128)(2,1)S(1)} %pad_maximum_fusion), channel_id=1, replica_groups=mesh['rep'=4,'fs'=4,'tp'=2] {'rep'}, use_global_device_ids=true, to_apply=%region_10.0 | all-reduce | flops 4608 | bytes 18432 | tf_op jit(solution)/shard_map/psum | solution.py:84
  173.5 0.6 convert_element_type.86
  174.1 146.8 %all-reduce.12.cloned.1.call-done = (bf16[512,1536]{0,1:T(8,128)(2,1)}, bf16[512,1536]{0,1:T(8,128)(2,1)}, bf16[1536,512]{1,0:T(8,128)(2,1)}) async-done(((bf16[512,1536]{0,1:T(8,128)(2,1)}, bf16[512,1536]{0,1:T(8,128)(2,1)}, bf16[1536,512]{1,0:T(8,128)(2,1)}), (bf16[512,1536]{0,1:T(8,128)(2,1)}, bf16[512,1536]{0,1:T(8,128)(2,1)}, bf16[1536,512]{1,0:T(8,128)(2,1)})) %all-reduce.12.cloned.1.call-update) | async-done | bytes 4718608 | tf_op jit(solution)/shard_map/psum | solution.py:81
  320.9 3.1 copy.14
  324.0 3.2 copy.15
  327.2 1.8 multiply_reduce_fusion.1
  329.0 0.4 multiply_reduce_fusion.2
  329.4 3.0 all-reduce.4
  332.5 3.4 multiply_reduce_fusion
  335.8 10.5 %psum.79 = f32[1536]{0:T(1024)} all-reduce(f32[1536]{0:T(1024)S(1)} %get-tuple-element.30), channel_id=1, replica_groups=mesh['rep'=4,'fs'=4,'tp'=2] {'fs'}, use_global_device_ids=true, to_apply=%region_16.0 | all-reduce | flops 1536 | bytes 12288 | tf_op jit(solution)/shard_map/psum | solution.py:34
  (18 shorter events, 0.1 us)
Async XLA Ops:
  7.2 1.4 copy-start
  7.2 4.6 %copy-start.8 = (bf16[512,1536]{1,0:T(8,128)(2,1)S(1)}, bf16[512,1536]{1,0:T(8,128)(2,1)}, u32[]{:S(2)}) copy-start(bf16[512,1536]{1,0:T(8,128)(2,1)} %param.8) | copy-start | bytes 4718596
  7.2 124.1 %all-reduce.10.cloned.1.call-start = ((), (), s32[]{:S(2)}) async-start(), calls=%async_computation.2 | async-start | bytes 9437184 | tf_op jit(solution)/shard_map/psum | solution.py:44
  8.6 3.2 copy-start.12
  11.8 2.1 copy-start.7
  11.8 2.2 copy-start.10
  16.1 0.7 copy-start.6
  16.2 304.8 %all-reduce.12.cloned.1.call-start = ((), (), s32[]{:S(2)}) async-start(), calls=%async_computation.3 | async-start | bytes 9437184 | tf_op jit(solution)/shard_map/psum | solution.py:81
  131.3 1.9 copy-start.1
  133.3 1.4 copy-start.2
  133.3 1.9 copy-start.4
  138.7 1.0 copy-start.11
  142.1 1.9 copy-start.13
  144.1 2.2 copy-start.5
  148.4 197.9 %reduce-scatter.2.cloned.1.call-start = ((), (), s32[]{:S(2)}) async-start(), calls=%async_computation.1 | async-start | bytes 786432 | tf_op jit(solution)/shard_map/reduce_scatter | solution.py:68
  148.5 2.5 copy-start.9
  324.0 5.0 %copy-start.3 = (bf16[512,1536]{0,1:T(8,128)(2,1)S(1)}, bf16[512,1536]{0,1:T(8,128)(2,1)}, u32[]{:S(2)}) copy-start(bf16[512,1536]{0,1:T(8,128)(2,1)} %get-tuple-element.27) | copy-start | bytes 4718596
Sparse Core Ops, SparseCore 0:
  16.3 115.0 all-reduce.9
  148.6 172.3 all-reduce.11
  323.8 6.8 reduce-scatter.1
where the time goes:
time: 353 us
  waiting for transfers between devices  261 us (74%)
  blocking collectives  34.1 us (10%)
  matrix products  18.6 us (5%)
  between operations  13.9 us (4%)
  local copies, waits for them, and re-layouts  13.5 us (4%)
  other arithmetic  11.3 us (3%)
    psum x1, waiting for transfers between devices, shards(): lax.psum(grad_gate.astype(jnp.bfloat16), 'rep').astype(jnp.float32)  147 us
    psum x1, waiting for transfers between devices, shards(): lax.psum(gate_part.astype(jnp.bfloat16), 'fs').astype(jnp.float32)  114 us
    psum x1, blocking collectives, shards(): lax.psum(grad_taps.astype(jnp.bfloat16), 'rep').astype(jnp.float32)  20.6 us
    dot_general x6, matrix products, contract(): lax.dot_general(left, right, (((left_dim,), (right_dim,)), ((), ())), pre...  13.2 us
    psum x1, blocking collectives, row_norms(): down_rows = lax.psum(down_rows, 'fs')  10.5 us
    unnamed x30, local copies, waits for them, and re-layouts  10.4 us
  transfers between devices with their start and end apart: 3, of which 2 were waited for; matrix products, arithmetic and copies ran while one was open for 5% of the time, Pallas kernels for 0%

commit v1 on v0

--- a/solution.py
+++ b/solution.py
@@ -1,6 +1,10 @@
+import functools
+
 import jax
 import jax.numpy as jnp
 from jax import lax
+from jax.experimental import pallas as pl
+from jax.experimental.pallas import tpu as pltpu
 from jax.sharding import PartitionSpec as P
 
 KW = 3
@@ -89,9 +93,434 @@
     return (in_grad, grad_gate, grad_up, grad_down, grad_taps, gate_rows, up_rows, down_rows)
 
 
+LANES = 128
+MID_LAG = 3
+OUT_LAG = 8
+MESH_ID = pl.DeviceIdType.MESH
+
+
+def layer_kernel(
+    n_rep, n_fs,
+    x_ref, wg_ref, wu_ref, taps_ref, wd_ref, og_ref,
+    in_grad_ref, pieces_ref, taps_out_ref, rows_gu_ref, rows_down_ref,
+    xt, send_part, recv_part, h_all, g_all, u_all, part, from_out, from_in, tot,
+    acc, ig_send, ig_recv, tap_all, tap_out, tap_in, rows, rows_tp, rows_fs,
+    rs_send, rs_recv, ag_send, ag_recv, a_send, out_recv, in_recv, b_send, loc_sem, misc,
+):
+    tok, feat = x_ref.shape
+    cw = n_fs * LANES
+    chunks = wg_ref.shape[1] // cw
+    subs = n_fs
+    total_pieces = chunks * 3 * subs
+    f32, bf16 = jnp.float32, jnp.bfloat16
+    r = lax.axis_index("rep")
+    f = lax.axis_index("fs")
+    t = lax.axis_index("tp")
+    half_rep = n_rep // 2
+    is_left = r < half_rep
+    toward = jnp.where(is_left, r + 1, r - 1)
+    outward = jnp.where(is_left, r - 1, r + 1)
+    is_end = jnp.logical_or(r == 0, r == n_rep - 1)
+    not_end = jnp.logical_not(is_end)
+    is_mid = jnp.logical_or(r == half_rep - 1, r == half_rep)
+    not_mid = jnp.logical_not(is_mid)
+    peers = [lax.rem(f + k, n_fs) for k in range(1, n_fs)]
+    own_cols = pl.ds(pl.multiple_of(f * LANES, LANES), LANES)
+
+    barrier = pltpu.get_barrier_semaphore()
+    for k in range(n_fs - 1):
+        pl.semaphore_signal(barrier, inc=1, device_id={"fs": peers[k]}, device_id_type=MESH_ID)
+    pl.semaphore_signal(barrier, inc=1, device_id={"tp": 1 - t}, device_id_type=MESH_ID)
+    pl.semaphore_signal(barrier, inc=1, device_id={"rep": toward}, device_id_type=MESH_ID)
+
+    @pl.when(not_end)
+    def _():
+        pl.semaphore_signal(barrier, inc=1, device_id={"rep": outward}, device_id_type=MESH_ID)
+
+    pl.semaphore_wait(barrier, n_fs + 1 + jnp.where(not_end, 1, 0))
+
+    def remote(src, dst, send, recv, device):
+        return pltpu.make_async_remote_copy(
+            src_ref=src, dst_ref=dst, send_sem=send, recv_sem=recv,
+            device_id=device, device_id_type=MESH_ID,
+        )
+
+    sent = []
+
+    def rs_copy(c, tensor, k):
+        s = (c * 3 + tensor) * (n_fs - 1) + k
+        return remote(
+            send_part.at[c, tensor, peers[k]], recv_part.at[c, tensor, k],
+            rs_send.at[s], rs_recv.at[s], {"fs": peers[k]},
+        )
+
+    def reduce_start(c):
+        cols = slice(c * cw, (c + 1) * cw)
+        for tensor in range(3):
+            if tensor == 0:
+                value = jnp.dot(x_ref[...], wg_ref[:, cols], preferred_element_type=f32)
+            elif tensor == 1:
+                value = jnp.dot(x_ref[...], wu_ref[:, cols], preferred_element_type=f32)
+            else:
+                value = contract(og_ref[...], wd_ref[cols, :], 1, 1)
+            value = value.astype(bf16)
+            for g in range(n_fs):
+                send_part[c, tensor, g] = value[:, g * LANES : (g + 1) * LANES]
+            for k in range(n_fs - 1):
+                copy = rs_copy(c, tensor, k)
+                copy.start()
+                sent.append(copy)
+
+    def reduced(c, tensor):
+        value = send_part[c, tensor, f].astype(f32)
+        for k in range(n_fs - 1):
+            rs_copy(c, tensor, k).wait_recv()
+            value = value + recv_part[c, tensor, k].astype(f32)
+        return value.astype(bf16).astype(f32)
+
+    def ag_copy(c, tensor, k):
+        s = (c * 3 + tensor) * (n_fs - 1) + k
+        if tensor == 0:
+            ref = h_all.at[c, f]
+        elif tensor == 1:
+            ref = g_all.at[c, :, own_cols]
+        else:
+            ref = u_all.at[c, :, own_cols]
+        return remote(ref, ref, ag_send.at[s], ag_recv.at[s], {"fs": peers[k]})
+
+    def gather_start(c, tensor):
+        for k in range(n_fs - 1):
+            copy = ag_copy(c, tensor, k)
+            copy.start()
+            sent.append(copy)
+
+    row_ids = lax.broadcasted_iota(jnp.int32, (tok, LANES), 0)
+
+    def down(value, lag):
+        if lag == 0:
+            return value
+        return jnp.where(row_ids >= lag, pltpu.roll(value, lag, 0), 0.0)
+
+    def up(value, lag):
+        if lag == 0:
+            return value
+        return jnp.where(row_ids < tok - lag, pltpu.roll(value, tok - lag, 0), 0.0)
+
+    def elementwise(c):
+        cols = pl.ds(pl.multiple_of(c * cw + f * LANES, LANES), LANES)
+        weights = taps_ref[:, cols].astype(f32)
+        gate = reduced(c, 0)
+        pre = weights[0:1] * down(gate, KW - 1)
+        for j in range(1, KW):
+            pre = pre + weights[j : j + 1] * down(gate, KW - 1 - j)
+        sig = 1.0 / (1.0 + jnp.exp(-pre))
+        silu = pre * sig
+        up_val = reduced(c, 1)
+        h_all[c, f] = (silu * up_val).T.astype(bf16)
+        gather_start(c, 0)
+        act = reduced(c, 2)
+        pre_grad = act * up_val * sig * (1.0 + pre * (1.0 - sig))
+        grad = weights[0:1] * up(pre_grad, KW - 1)
+        for j in range(1, KW):
+            grad = grad + weights[j : j + 1] * up(pre_grad, KW - 1 - j)
+        g_all[c, :, own_cols] = grad.astype(bf16)
+        gather_start(c, 1)
+        u_all[c, :, own_cols] = (act * silu).astype(bf16)
+        gather_start(c, 2)
+        for j in range(KW):
+            tap_all[f, c * 8 + j : c * 8 + j + 1, :] = jnp.sum(
+                down(gate, KW - 1 - j) * pre_grad, axis=0, keepdims=True
+            )
+
+    def part_copy(p):
+        return remote(part.at[p], from_out.at[p], a_send.at[p], out_recv.at[p], {"rep": toward})
+
+    def exchange_copy(p):
+        return remote(part.at[p], from_in.at[p], a_send.at[p], in_recv.at[p], {"rep": toward})
+
+    def total_copy(p, src):
+        return remote(src.at[p], from_in.at[p], b_send.at[p], in_recv.at[p], {"rep": outward})
+
+    def local_copy(p, src):
+        return pltpu.make_async_copy(src.at[p], pieces_ref.at[p], loc_sem.at[p])
+
+    def stage_a(p, value):
+        @pl.when(not_end)
+        def _():
+            part_copy(p).wait_recv()
+            part[p] = (value + from_out[p].astype(f32)).astype(bf16)
+
+        @pl.when(is_end)
+        def _():
+            part[p] = value.astype(bf16)
+
+        @pl.when(is_mid)
+        def _():
+            exchange_copy(p).start()
+
+        @pl.when(not_mid)
+        def _():
+            part_copy(p).start()
+
+    def norms(p, value):
+        square = value * value
+        lanes = square[:, :LANES]
+        for g in range(1, square.shape[1] // LANES):
+            lanes = lanes + square[:, g * LANES : (g + 1) * LANES]
+        rows[pl.ds(p, 1), :] = jnp.sum(lanes.T, axis=0, keepdims=True)
+
+    def stage_b_mid(p):
+        exchange_copy(p).wait_recv()
+        value = (part[p].astype(f32) + from_in[p].astype(f32)).astype(bf16)
+        tot[p] = value
+
+        @pl.when(not_end)
+        def _():
+            total_copy(p, tot).start()
+
+        local_copy(p, tot).start()
+        norms(p, value.astype(f32))
+
+    def stage_b_out(p):
+        exchange_copy(p).wait_recv()
+
+        @pl.when(not_end)
+        def _():
+            total_copy(p, from_in).start()
+
+        local_copy(p, from_in).start()
+        norms(p, from_in[p].astype(f32))
+
+    def stage_b(slot):
+        @pl.when(jnp.logical_and(is_mid, jnp.logical_and(slot >= MID_LAG, slot < total_pieces + MID_LAG)))
+        def _():
+            stage_b_mid(slot - MID_LAG)
+
+        @pl.when(jnp.logical_and(not_mid, slot >= OUT_LAG))
+        def _():
+            stage_b_out(slot - OUT_LAG)
+
+    def segment(c, tensor):
+        for k in range(n_fs - 1):
+            ag_copy(c, tensor, k).wait_recv()
+
+        @pl.loop(0, subs)
+        def _(q):
+            p = (c * 3 + tensor) * subs + q
+            if tensor == 0:
+                value = jnp.dot(h_all[c, q], og_ref[...], preferred_element_type=f32)
+            elif tensor == 1:
+                value = jnp.dot(xt[q], g_all[c], preferred_element_type=f32)
+            else:
+                value = jnp.dot(xt[q], u_all[c], preferred_element_type=f32)
+            stage_a(p, value)
+            stage_b(p)
+
+    def input_term(c):
+        cols = slice(c * cw, (c + 1) * cw)
+        term = contract(g_all[c], wg_ref[:, cols], 1, 1) + contract(u_all[c], wu_ref[:, cols], 1, 1)
+        if c == 0:
+            acc[...] = term
+        else:
+            acc[...] += term
+
+    tap_all[...] = jnp.zeros_like(tap_all)
+    reduce_start(0)
+    for q in range(feat // LANES):
+        xt[q] = x_ref[:, q * LANES : (q + 1) * LANES].astype(f32).T.astype(bf16)
+    elementwise(0)
+    if chunks > 1:
+        reduce_start(1)
+    tap_peers = []
+    for c in range(chunks):
+        segment(c, 0)
+        segment(c, 1)
+        if c + 1 < chunks:
+            elementwise(c + 1)
+            if c + 2 < chunks:
+                reduce_start(c + 2)
+        else:
+            for k in range(n_fs - 1):
+                copy = remote(
+                    tap_all.at[f], tap_all.at[f], misc.at[2 * k], misc.at[2 * k + 1], {"fs": peers[k]}
+                )
+                copy.start()
+                tap_peers.append(copy)
+        segment(c, 2)
+        input_term(c)
+
+    m = 2 * (n_fs - 1)
+    half = tok // 2
+    ig_send[...] = acc[...].astype(bf16)
+    ig_copy = remote(
+        ig_send.at[pl.ds(pl.multiple_of((1 - t) * half, half), half)], ig_recv,
+        misc.at[m], misc.at[m + 1], {"tp": 1 - t},
+    )
+    ig_copy.start()
+
+    for copy in tap_peers:
+        copy.wait()
+    tap_part = remote(tap_all, tap_out, misc.at[m + 2], misc.at[m + 3], {"rep": toward})
+    tap_exchange = remote(tap_all, tap_in, misc.at[m + 2], misc.at[m + 4], {"rep": toward})
+    tap_total = remote(taps_out_ref, tap_in, misc.at[m + 5], misc.at[m + 4], {"rep": outward})
+
+    @pl.when(not_end)
+    def _():
+        tap_part.wait_recv()
+        tap_all[...] = tap_all[...] + tap_out[...]
+
+    @pl.when(is_mid)
+    def _():
+        tap_exchange.start()
+
+    @pl.when(not_mid)
+    def _():
+        tap_part.start()
+
+    ig_copy.wait()
+    in_grad_ref[...] = (
+        ig_send[pl.ds(pl.multiple_of(t * half, half), half), :].astype(f32) + ig_recv[...].astype(f32)
+    ).astype(bf16)
+
+    @pl.loop(total_pieces, total_pieces + OUT_LAG)
+    def _(slot):
+        stage_b(slot)
+
+    tap_exchange.wait_recv()
+
+    @pl.when(is_mid)
+    def _():
+        taps_out_ref[...] = tap_all[...] + tap_in[...]
+
+    @pl.when(not_mid)
+    def _():
+        taps_out_ref[...] = tap_in[...]
+
+    @pl.when(not_end)
+    def _():
+        tap_total.start()
+
+    rows_copies = [
+        remote(rows, rows_tp, misc.at[m + 6], misc.at[m + 7], {"tp": 1 - t})
+    ]
+    for k in range(n_fs - 1):
+        rows_copies.append(
+            remote(rows, rows_fs.at[k], misc.at[m + 8 + 2 * k], misc.at[m + 9 + 2 * k], {"fs": peers[k]})
+        )
+    for copy in rows_copies:
+        copy.start()
+
+    for copy in sent:
+        copy.wait_send()
+    tap_part.wait_send()
+
+    @pl.loop(0, total_pieces)
+    def _(p):
+        part_copy(p).wait_send()
+
+        @pl.when(not_end)
+        def _():
+            total_copy(p, tot).wait_send()
+
+        local_copy(p, tot).wait()
+
+    for copy in rows_copies:
+        copy.wait()
+    for tensor in (1, 2):
+        value = jnp.zeros((subs, LANES), f32)
+        for c in range(chunks):
+            at = (c * 3 + tensor) * subs
+            value = value + (rows[at : at + subs, :] + rows_tp[at : at + subs, :])
+        rows_gu_ref[(tensor - 1) * subs : tensor * subs, :] = value
+    for c in range(chunks):
+        at = c * 3 * subs
+        value = rows[at : at + subs, :]
+        for k in range(n_fs - 1):
+            value = value + rows_fs[k, at : at + subs, :]
+        rows_down_ref[c * subs : (c + 1) * subs, :] = value
+
+    @pl.when(not_end)
+    def _():
+        tap_total.wait_send()
+
+
+def fits(shape, inputs, w_gate):
+    n_rep, n_fs, n_tp = shape["rep"], shape["fs"], shape["tp"]
+    tok, feat = inputs.shape
+    cw = n_fs * LANES
+    return (
+        n_rep == 4 and n_fs == 4 and n_tp == 2 and feat == cw
+        and w_gate.shape[1] % cw == 0 and w_gate.shape[1] <= 1536 and tok % LANES == 0 and tok <= 512
+    )
+
+
+def fused_shards(shape, inputs, w_gate, w_up, conv_taps, w_down, out_grad):
+    if not fits(shape, inputs, w_gate):
+        return shards(inputs, w_gate, w_up, conv_taps, w_down, out_grad)
+    n_rep, n_fs = shape["rep"], shape["fs"]
+    tok, feat = inputs.shape
+    hid = w_gate.shape[1]
+    cw = n_fs * LANES
+    chunks = hid // cw
+    subs = n_fs
+    pieces = chunks * 3 * subs
+    bf16, f32 = jnp.bfloat16, jnp.float32
+    vmem = pl.BlockSpec(memory_space=pltpu.VMEM)
+    hops = chunks * 3 * (n_fs - 1)
+    dma = pltpu.SemaphoreType.DMA
+    in_grad, grads, taps, rows_gu, rows_down = pl.pallas_call(
+        functools.partial(layer_kernel, n_rep, n_fs),
+        out_shape=(
+            jax.ShapeDtypeStruct((tok // 2, feat), bf16),
+            jax.ShapeDtypeStruct((pieces, LANES, cw), bf16),
+            jax.ShapeDtypeStruct((n_fs, chunks * 8, LANES), f32),
+            jax.ShapeDtypeStruct((2 * subs, LANES), f32),
+            jax.ShapeDtypeStruct((chunks * subs, LANES), f32),
+        ),
+        in_specs=[vmem] * 6,
+        out_specs=(vmem, pl.BlockSpec(memory_space=pl.ANY), vmem, vmem, vmem),
+        scratch_shapes=[
+            pltpu.VMEM((subs, LANES, tok), bf16),
+            pltpu.VMEM((chunks, 3, n_fs, tok, LANES), bf16),
+            pltpu.VMEM((chunks, 3, n_fs - 1, tok, LANES), bf16),
+            pltpu.VMEM((chunks, n_fs, LANES, tok), bf16),
+            pltpu.VMEM((chunks, tok, cw), bf16),
+            pltpu.VMEM((chunks, tok, cw), bf16),
+            pltpu.VMEM((pieces, LANES, cw), bf16),
+            pltpu.VMEM((pieces, LANES, cw), bf16),
+            pltpu.VMEM((pieces, LANES, cw), bf16),
+            pltpu.VMEM((pieces, LANES, cw), bf16),
+            pltpu.VMEM((tok, feat), f32),
+            pltpu.VMEM((tok, feat), bf16),
+            pltpu.VMEM((tok // 2, feat), bf16),
+            pltpu.VMEM((n_fs, chunks * 8, LANES), f32),
+            pltpu.VMEM((n_fs, chunks * 8, LANES), f32),
+            pltpu.VMEM((n_fs, chunks * 8, LANES), f32),
+            pltpu.VMEM((pieces, LANES), f32),
+            pltpu.VMEM((pieces, LANES), f32),
+            pltpu.VMEM((n_fs - 1, pieces, LANES), f32),
+            dma((hops,)), dma((hops,)), dma((hops,)), dma((hops,)),
+            dma((pieces,)), dma((pieces,)), dma((pieces,)), dma((pieces,)), dma((pieces,)),
+            dma((4 * (n_fs - 1) + 8,)),
+        ],
+        compiler_params=pltpu.CompilerParams(
+            collective_id=0, has_side_effects=True, vmem_limit_bytes=60 * 1024 * 1024
+        ),
+    )(inputs, w_gate, w_up, conv_taps, w_down, out_grad)
+    grads = grads.reshape(chunks, 3, subs, LANES, cw)
+    grad_down = grads[:, 0].reshape(hid, feat).astype(f32)
+    grad_gate = grads[:, 1].transpose(1, 2, 0, 3).reshape(feat, hid).astype(f32)
+    grad_up = grads[:, 2].transpose(1, 2, 0, 3).reshape(feat, hid).astype(f32)
+    grad_taps = taps.reshape(n_fs, chunks, 8, LANES)[:, :, :KW].transpose(2, 1, 0, 3).reshape(KW, hid)
+    return (
+        in_grad, grad_gate, grad_up, grad_down, grad_taps,
+        rows_gu[:subs].reshape(feat), rows_gu[subs:].reshape(feat), rows_down.reshape(hid),
+    )
+
+
 def solution(mesh):
     return jax.shard_map(
-        shards,
+        functools.partial(fused_shards, dict(mesh.shape)),
         mesh=mesh,
         in_specs=(
             P("rep", "fs"),

time: 353 us -> 194 us (0.55)
  waiting for transfers between devices: 261 us -> 0 us
  Pallas kernels: 0 us -> 163 us
  blocking collectives: 34.1 us -> 0 us
  matrix products: 18.6 us -> 0 us
  between operations: 13.9 us -> 0.67 us
  local copies, waits for them, and re-layouts: 13.5 us -> 21.6 us
    psum x2 -> x0, waiting for transfers between devices: 261 us -> none  [the longest x1 147 us: shards(): lax.psum(grad_gate.astype(jnp.bfloat16), 'rep').astype(jnp.float32)]
    pallas_call x0 -> x1, Pallas kernels: none -> 163 us  [fused_shards(): pl.pallas_call(functools.partial(layer_kernel, n_rep, n_fs), out_shape=(j...]
    psum x3 -> x0, blocking collectives: 34.1 us -> none  [the longest x1 20.6 us: shards(): lax.psum(grad_taps.astype(jnp.bfloat16), 'rep').astype(jnp.float32)]
    dot_general x8 -> x0, matrix products: 18.6 us -> none  [the longest x6 13.2 us: contract(): lax.dot_general(left, right, (((left_dim,), (right_dim,)), ((), ())), pre...]
    reduce_sum x4 -> x0, other arithmetic: 8.74 us -> none  [the longest x1 3.37 us: row_norms(): down_rows = jnp.sum(grad_down * grad_down, axis=1)]
    unnamed x30 -> x12, local copies, waits for them, and re-layouts: 10.4 us -> 18.8 us
    slice x0 -> x1, other arithmetic: none -> 6.02 us  [fused_shards(): grad_down = grads[:, 0].reshape(hid, feat).astype(f32)]
  transfers between devices with their start and end apart: 3 -> 0, of which waited for: 2 -> 0; matrix products, arithmetic and copies ran while one was open for 5% -> 0% of each run, Pallas kernels for 0% -> 0%
where the time goes in v1:
time: 194 us
  Pallas kernels  163 us (84%)
  local copies, waits for them, and re-layouts  21.6 us (11%)
  other arithmetic  8.23 us (4%)
    pallas_call x1, Pallas kernels, fused_shards(): pl.pallas_call(functools.partial(layer_kernel, n_rep, n_fs), out_shape=(j...  163 us
    unnamed x12, local copies, waits for them, and re-layouts  18.8 us
    slice x1, other arithmetic, fused_shards(): grad_down = grads[:, 0].reshape(hid, feat).astype(f32)  6.02 us

profile of v1, /device:TPU:0, one launch (start us, length us, event | category | flops | bytes accessed | tf_op | source)
XLA Modules:
  0.0 193.6 jit_solution(12212205278335989183)
XLA Ops:
  0.6 163.1 %shard_map.125 = (bf16[256,512]{1,0:T(8,128)(2,1)}, bf16[36,128,512]{2,1,0:T(8,128)(2,1)}, f32[4,24,128]{2,1,0:T(8,128)}, f32[8,128]{1,0:T(8,128)}, f32[12,128]{1,0:T(8,128)}) custom-call(bf16[512,512]{1,0:T(8,128)(2,1)} %x_ref.1, bf16[512,1536]{1,0:T(8,128)(2,1)} %wg_ref.1, bf16[512,1536]{1,0:T(8,128)(2,1)} %wu_ref.1, bf16[3,1536]{1,0:T(4,128)(2,1)} %taps_ref.1, ...), custom_call_target="tpu_custom_call" | custom-call | tf_op jit(solution)/shard_map/pallas_call | solution.py:471
  163.7 1.3 slice_bitcast_fusion.1
  165.1 0.8 slice_bitcast_fusion
  165.9 0.6 reshape.48
  166.5 6.0 %fusion = (bf16[3,1,4,128,512]{4,3,2,1,0:T(8,128)(2,1)S(1)}, f32[3,1,4,128,512]{4,3,2,1,0:T(8,128)}, f32[3,1,4,128,512]{4,3,2,1,0:T(8,128)}) fusion(bf16[3,3,4,128,512]{4,3,2,1,0:T(8,128)(2,1)} %bitcast.40), kind=kLoop, calls=%fused_computation.8 | loop fusion | flops 1572864 | bytes 12582912 | tf_op jit(solution)/shard_map/slice | solution.py:511
  172.5 2.2 %bitcast_convert_fusion = f32[1536,512]{1,0:T(8,128)} fusion(bf16[3,1,4,128,512]{4,3,2,1,0:T(8,128)(2,1)S(1)} %get-tuple-element.26), kind=kLoop, calls=%fused_computation.4 | loop fusion | flops 786432 | bytes 4718592 | tf_op jit(solution)/shard_map/convert_element_type | solution.py:511
  174.7 3.2 %copy.26 = f32[3,1,4,128,512]{3,2,4,0,1:T(4,128)S(1)} copy(f32[3,1,4,128,512]{4,3,2,1,0:T(8,128)} %get-tuple-element.27) | data formatting | bytes 6291456
  178.0 2.0 %copy.31 = f32[192,8,4,128]{3,1,2,0:T(8,128)} copy(f32[192,8,4,128]{3,2,1,0:T(4,128)S(1)} %bitcast.36) | data formatting | bytes 6291456
  180.0 3.5 %copy.20 = f32[512,1536]{1,0:T(8,128)} copy(f32[512,1536]{0,1:T(8,128)} %bitcast.37) | data formatting | bytes 6291456
  183.5 3.2 %copy.27 = f32[3,1,4,128,512]{3,2,4,0,1:T(4,128)S(1)} copy(f32[3,1,4,128,512]{4,3,2,1,0:T(8,128)} %get-tuple-element.28) | data formatting | bytes 6291456
  186.7 1.9 %copy.30 = f32[192,8,4,128]{3,1,2,0:T(8,128)} copy(f32[192,8,4,128]{3,2,1,0:T(4,128)S(1)} %bitcast.38) | data formatting | bytes 6291456
  188.7 0.0 copy-start
  188.7 0.0 copy-start.1
  188.7 3.6 %copy.21 = f32[512,1536]{1,0:T(8,128)} copy(f32[512,1536]{0,1:T(8,128)} %bitcast.39) | data formatting | bytes 6291456
  192.3 0.0 copy-done
  192.3 0.7 copy.34
  193.0 0.0 copy-done.1
  193.0 0.6 copy.35
  (1 shorter events, 0.0 us)
Async XLA Ops:
  188.7 3.6 %copy-start = (bf16[256,512]{1,0:T(8,128)(2,1)S(1)}, bf16[256,512]{1,0:T(8,128)(2,1)}, u32[]{:S(2)}) copy-start(bf16[256,512]{1,0:T(8,128)(2,1)} %get-tuple-element.39) | copy-start | bytes 786436
  188.7 4.3 %copy-start.1 = (f32[12,128]{1,0:T(8,128)S(1)}, f32[12,128]{1,0:T(8,128)}, u32[]{:S(2)}) copy-start(f32[12,128]{1,0:T(8,128)} %get-tuple-element.17) | copy-start | bytes 18436

commit v2 on v1

--- a/solution.py
+++ b/solution.py
@@ -94,6 +94,8 @@
 
 
 LANES = 128
+CW = 256
+HALO = 16
 MID_LAG = 3
 OUT_LAG = 8
 MESH_ID = pl.DeviceIdType.MESH
@@ -102,15 +104,17 @@
 def layer_kernel(
     n_rep, n_fs,
     x_ref, wg_ref, wu_ref, taps_ref, wd_ref, og_ref,
-    in_grad_ref, pieces_ref, taps_out_ref, rows_gu_ref, rows_down_ref,
+    in_grad_ref, down_ref, gate_ref, up_ref, taps_out_ref, rows_gate_ref, rows_up_ref, rows_down_ref,
     xt, send_part, recv_part, h_all, g_all, u_all, part, from_out, from_in, tot,
-    acc, ig_send, ig_recv, tap_all, tap_out, tap_in, rows, rows_tp, rows_fs,
+    acc, ig_send, ig_recv, tap_all, tap_out, tap_in, tap_sum, rows, rows_tp, rows_fs,
     rs_send, rs_recv, ag_send, ag_recv, a_send, out_recv, in_recv, b_send, loc_sem, misc,
 ):
     tok, feat = x_ref.shape
-    cw = n_fs * LANES
+    cw = CW
     chunks = wg_ref.shape[1] // cw
-    subs = n_fs
+    subs = feat // cw
+    own_rows = tok // 2
+    span = own_rows + HALO
     total_pieces = chunks * 3 * subs
     f32, bf16 = jnp.float32, jnp.bfloat16
     r = lax.axis_index("rep")
@@ -124,8 +128,14 @@
     not_end = jnp.logical_not(is_end)
     is_mid = jnp.logical_or(r == half_rep - 1, r == half_rep)
     not_mid = jnp.logical_not(is_mid)
-    peers = [lax.rem(f + k, n_fs) for k in range(1, n_fs)]
-    own_cols = pl.ds(pl.multiple_of(f * LANES, LANES), LANES)
+    beside = f + 1 - 2 * lax.rem(f, 2)
+    across = lax.rem(f + 2, 4)
+    corner = lax.rem(beside + 2, 4)
+    peers = [beside, across, corner]
+    side = lax.rem(f, 2)
+    top = f // 2
+    own_cols = pl.ds(pl.multiple_of(side * LANES, LANES), LANES)
+    own_toks = pl.ds(pl.multiple_of(top * own_rows, own_rows), own_rows)
 
     barrier = pltpu.get_barrier_semaphore()
     for k in range(n_fs - 1):
@@ -165,7 +175,9 @@
                 value = contract(og_ref[...], wd_ref[cols, :], 1, 1)
             value = value.astype(bf16)
             for g in range(n_fs):
-                send_part[c, tensor, g] = value[:, g * LANES : (g + 1) * LANES]
+                first = (g // 2) * (own_rows - HALO)
+                lane = (g % 2) * LANES
+                send_part[c, tensor, g] = value[first : first + span, lane : lane + LANES]
             for k in range(n_fs - 1):
                 copy = rs_copy(c, tensor, k)
                 copy.start()
@@ -178,23 +190,56 @@
             value = value + recv_part[c, tensor, k].astype(f32)
         return value.astype(bf16).astype(f32)
 
-    def ag_copy(c, tensor, k):
-        s = (c * 3 + tensor) * (n_fs - 1) + k
+    def block(c, tensor, owner, part_of=None):
+        col = lax.rem(owner, 2) * LANES
+        row = (owner // 2) * own_rows
         if tensor == 0:
-            ref = h_all.at[c, f]
-        elif tensor == 1:
-            ref = g_all.at[c, :, own_cols]
+            size = LANES if part_of is None else LANES // 2
+            start = col + (0 if part_of is None else part_of * size)
+            return h_all.at[
+                c, pl.ds(pl.multiple_of(start, size), size), pl.ds(pl.multiple_of(row, own_rows), own_rows)
+            ]
+        size = own_rows if part_of is None else own_rows // 2
+        start = row + (0 if part_of is None else part_of * size)
+        ref = g_all if tensor == 1 else u_all
+        return ref.at[c, pl.ds(pl.multiple_of(start, size), size), pl.ds(pl.multiple_of(col, LANES), LANES)]
+
+    def ag_copy(c, tensor, step, owner):
+        s = (c * 3 + tensor) * 4
+        if step == 0:
+            ref, slot, target = block(c, tensor, owner), 0, beside
+        elif step == 1:
+            ref, slot, target = block(c, tensor, owner), 1, across
+        elif step == 2:
+            ref, slot, target = block(c, tensor, owner, 1), 2, beside
         else:
-            ref = u_all.at[c, :, own_cols]
-        return remote(ref, ref, ag_send.at[s], ag_recv.at[s], {"fs": peers[k]})
+            ref, slot, target = block(c, tensor, owner, 0), 3, across
+        return remote(ref, ref, ag_send.at[s + slot], ag_recv.at[s + slot], {"fs": target})
 
     def gather_start(c, tensor):
-        for k in range(n_fs - 1):
-            copy = ag_copy(c, tensor, k)
+        for step in (0, 1):
+            copy = ag_copy(c, tensor, step, f)
             copy.start()
             sent.append(copy)
 
-    row_ids = lax.broadcasted_iota(jnp.int32, (tok, LANES), 0)
+    def forward(c, tensor):
+        ag_copy(c, tensor, 0, beside).wait_recv()
+        copy = ag_copy(c, tensor, 3, beside)
+        copy.start()
+        sent.append(copy)
+        ag_copy(c, tensor, 1, across).wait_recv()
+        copy = ag_copy(c, tensor, 2, across)
+        copy.start()
+        sent.append(copy)
+
+    def gathered(c, tensor):
+        ag_copy(c, tensor, 2, corner).wait_recv()
+        ag_copy(c, tensor, 3, corner).wait_recv()
+
+    def own(value):
+        return jnp.where(top == 0, value[:own_rows], value[HALO:])
+
+    row_ids = lax.broadcasted_iota(jnp.int32, (span, LANES), 0)
 
     def down(value, lag):
         if lag == 0:
@@ -204,10 +249,10 @@
     def up(value, lag):
         if lag == 0:
             return value
-        return jnp.where(row_ids < tok - lag, pltpu.roll(value, tok - lag, 0), 0.0)
+        return jnp.where(row_ids < span - lag, pltpu.roll(value, span - lag, 0), 0.0)
 
     def elementwise(c):
-        cols = pl.ds(pl.multiple_of(c * cw + f * LANES, LANES), LANES)
+        cols = pl.ds(pl.multiple_of(c * cw + side * LANES, LANES), LANES)
         weights = taps_ref[:, cols].astype(f32)
         gate = reduced(c, 0)
         pre = weights[0:1] * down(gate, KW - 1)
@@ -216,20 +261,20 @@
         sig = 1.0 / (1.0 + jnp.exp(-pre))
         silu = pre * sig
         up_val = reduced(c, 1)
-        h_all[c, f] = (silu * up_val).T.astype(bf16)
+        h_all[c, own_cols, own_toks] = own(silu * up_val).T.astype(bf16)
         gather_start(c, 0)
         act = reduced(c, 2)
         pre_grad = act * up_val * sig * (1.0 + pre * (1.0 - sig))
         grad = weights[0:1] * up(pre_grad, KW - 1)
         for j in range(1, KW):
             grad = grad + weights[j : j + 1] * up(pre_grad, KW - 1 - j)
-        g_all[c, :, own_cols] = grad.astype(bf16)
+        g_all[c, own_toks, own_cols] = own(grad).astype(bf16)
         gather_start(c, 1)
-        u_all[c, :, own_cols] = (act * silu).astype(bf16)
+        u_all[c, own_toks, own_cols] = own(act * silu).astype(bf16)
         gather_start(c, 2)
         for j in range(KW):
-            tap_all[f, c * 8 + j : c * 8 + j + 1, :] = jnp.sum(
-                down(gate, KW - 1 - j) * pre_grad, axis=0, keepdims=True
+            tap_all[f, c * KW + j : c * KW + j + 1, :] = jnp.sum(
+                own(down(gate, KW - 1 - j) * pre_grad), axis=0, keepdims=True
             )
 
     def part_copy(p):
@@ -241,8 +286,29 @@
     def total_copy(p, src):
         return remote(src.at[p], from_in.at[p], b_send.at[p], in_recv.at[p], {"rep": outward})
 
-    def local_copy(p, src):
-        return pltpu.make_async_copy(src.at[p], pieces_ref.at[p], loc_sem.at[p])
+    def local_copy(p, src, tensor, wait):
+        c = p // (3 * subs)
+        q = p % subs
+        along = pl.ds(pl.multiple_of(c * cw, cw), cw)
+        inner = pl.ds(pl.multiple_of(q * cw, cw), cw)
+        if tensor == 0:
+            dst = down_ref.at[along, inner]
+        elif tensor == 1:
+            dst = gate_ref.at[inner, along]
+        else:
+            dst = up_ref.at[inner, along]
+        copy = pltpu.make_async_copy(src.at[p], dst, loc_sem.at[p])
+        if wait:
+            copy.wait()
+        else:
+            copy.start()
+
+    def store_out(p, src, wait=False):
+        kind = (p // subs) % 3
+        for tensor in range(3):
+            @pl.when(kind == tensor)
+            def _(tensor=tensor):
+                local_copy(p, src, tensor, wait)
 
     def stage_a(p, value):
         @pl.when(not_end)
@@ -267,7 +333,10 @@
         lanes = square[:, :LANES]
         for g in range(1, square.shape[1] // LANES):
             lanes = lanes + square[:, g * LANES : (g + 1) * LANES]
-        rows[pl.ds(p, 1), :] = jnp.sum(lanes.T, axis=0, keepdims=True)
+        for i in range(cw // LANES):
+            rows[pl.ds(p * (cw // LANES) + i, 1), :] = jnp.sum(
+                lanes[i * LANES : (i + 1) * LANES].T, axis=0, keepdims=True
+            )
 
     def stage_b_mid(p):
         exchange_copy(p).wait_recv()
@@ -278,7 +347,7 @@
         def _():
             total_copy(p, tot).start()
 
-        local_copy(p, tot).start()
+        store_out(p, tot)
         norms(p, value.astype(f32))
 
     def stage_b_out(p):
@@ -288,7 +357,7 @@
         def _():
             total_copy(p, from_in).start()
 
-        local_copy(p, from_in).start()
+        store_out(p, from_in)
         norms(p, from_in[p].astype(f32))
 
     def stage_b(slot):
@@ -301,14 +370,15 @@
             stage_b_out(slot - OUT_LAG)
 
     def segment(c, tensor):
-        for k in range(n_fs - 1):
-            ag_copy(c, tensor, k).wait_recv()
+        gathered(c, tensor)
 
         @pl.loop(0, subs)
         def _(q):
             p = (c * 3 + tensor) * subs + q
             if tensor == 0:
-                value = jnp.dot(h_all[c, q], og_ref[...], preferred_element_type=f32)
+                value = jnp.dot(
+                    h_all[c], og_ref[:, pl.ds(pl.multiple_of(q * cw, cw), cw)], preferred_element_type=f32
+                )
             elif tensor == 1:
                 value = jnp.dot(xt[q], g_all[c], preferred_element_type=f32)
             else:
@@ -324,21 +394,19 @@
         else:
             acc[...] += term
 
-    tap_all[...] = jnp.zeros_like(tap_all)
     reduce_start(0)
-    for q in range(feat // LANES):
-        xt[q] = x_ref[:, q * LANES : (q + 1) * LANES].astype(f32).T.astype(bf16)
+    for q in range(subs):
+        xt[q] = x_ref[:, q * cw : (q + 1) * cw].astype(f32).T.astype(bf16)
     elementwise(0)
     if chunks > 1:
         reduce_start(1)
     tap_peers = []
-    for c in range(chunks):
-        segment(c, 0)
-        segment(c, 1)
-        if c + 1 < chunks:
-            elementwise(c + 1)
-            if c + 2 < chunks:
-                reduce_start(c + 2)
+
+    def advance(c):
+        if c < chunks:
+            elementwise(c)
+            if c + 1 < chunks:
+                reduce_start(c + 1)
         else:
             for k in range(n_fs - 1):
                 copy = remote(
@@ -346,7 +414,22 @@
                 )
                 copy.start()
                 tap_peers.append(copy)
+
+    forward(0, 0)
+    for c in range(chunks):
+        segment(c, 0)
+        if c > 0:
+            advance(c + 1)
+        forward(c, 1)
+        if c > 0:
+            forward(c, 2)
+        segment(c, 1)
+        if c == 0:
+            forward(c, 2)
+            advance(c + 1)
         segment(c, 2)
+        if c + 1 < chunks:
+            forward(c + 1, 0)
         input_term(c)
 
     m = 2 * (n_fs - 1)
@@ -362,7 +445,7 @@
         copy.wait()
     tap_part = remote(tap_all, tap_out, misc.at[m + 2], misc.at[m + 3], {"rep": toward})
     tap_exchange = remote(tap_all, tap_in, misc.at[m + 2], misc.at[m + 4], {"rep": toward})
-    tap_total = remote(taps_out_ref, tap_in, misc.at[m + 5], misc.at[m + 4], {"rep": outward})
+    tap_total = remote(tap_sum, tap_in, misc.at[m + 5], misc.at[m + 4], {"rep": outward})
 
     @pl.when(not_end)
     def _():
@@ -390,11 +473,11 @@
 
     @pl.when(is_mid)
     def _():
-        taps_out_ref[...] = tap_all[...] + tap_in[...]
+        tap_sum[...] = tap_all[...] + tap_in[...]
 
     @pl.when(not_mid)
     def _():
-        taps_out_ref[...] = tap_in[...]
+        tap_sum[...] = tap_in[...]
 
     @pl.when(not_end)
     def _():
@@ -422,22 +505,35 @@
         def _():
             total_copy(p, tot).wait_send()
 
-        local_copy(p, tot).wait()
+        store_out(p, tot, True)
 
     for copy in rows_copies:
         copy.wait()
-    for tensor in (1, 2):
-        value = jnp.zeros((subs, LANES), f32)
-        for c in range(chunks):
-            at = (c * 3 + tensor) * subs
-            value = value + (rows[at : at + subs, :] + rows_tp[at : at + subs, :])
-        rows_gu_ref[(tensor - 1) * subs : tensor * subs, :] = value
+    per = cw // LANES
+    for tensor, rows_ref in ((1, rows_gate_ref), (2, rows_up_ref)):
+        for q in range(subs):
+            for i in range(per):
+                value = jnp.zeros((1, LANES), f32)
+                for c in range(chunks):
+                    at = ((c * 3 + tensor) * subs + q) * per + i
+                    value = value + (rows[at : at + 1, :] + rows_tp[at : at + 1, :])
+                lane = (q * per + i) * LANES
+                rows_ref[:, lane : lane + LANES] = value
     for c in range(chunks):
-        at = c * 3 * subs
-        value = rows[at : at + subs, :]
-        for k in range(n_fs - 1):
-            value = value + rows_fs[k, at : at + subs, :]
-        rows_down_ref[c * subs : (c + 1) * subs, :] = value
+        for i in range(per):
+            value = jnp.zeros((1, LANES), f32)
+            for q in range(subs):
+                at = (c * 3 * subs + q) * per + i
+                value = value + rows[at : at + 1, :]
+                for k in range(n_fs - 1):
+                    value = value + rows_fs[k, at : at + 1, :]
+            lane = (c * per + i) * LANES
+            rows_down_ref[:, lane : lane + LANES] = value
+            for j in range(KW):
+                at = c * KW + j
+                taps_out_ref[j : j + 1, lane : lane + LANES] = (
+                    tap_sum[i, at : at + 1, :] + tap_sum[i + 2, at : at + 1, :]
+                )
 
     @pl.when(not_end)
     def _():
@@ -447,10 +543,9 @@
 def fits(shape, inputs, w_gate):
     n_rep, n_fs, n_tp = shape["rep"], shape["fs"], shape["tp"]
     tok, feat = inputs.shape
-    cw = n_fs * LANES
     return (
-        n_rep == 4 and n_fs == 4 and n_tp == 2 and feat == cw
-        and w_gate.shape[1] % cw == 0 and w_gate.shape[1] <= 1536 and tok % LANES == 0 and tok <= 512
+        n_rep == 4 and n_fs == 4 and n_tp == 2 and feat == 2 * CW
+        and w_gate.shape[1] % CW == 0 and w_gate.shape[1] <= 1536 and tok % LANES == 0 and tok <= 512
     )
 
 
@@ -460,46 +555,50 @@
     n_rep, n_fs = shape["rep"], shape["fs"]
     tok, feat = inputs.shape
     hid = w_gate.shape[1]
-    cw = n_fs * LANES
+    cw = CW
     chunks = hid // cw
-    subs = n_fs
+    subs = feat // cw
     pieces = chunks * 3 * subs
     bf16, f32 = jnp.bfloat16, jnp.float32
     vmem = pl.BlockSpec(memory_space=pltpu.VMEM)
     hops = chunks * 3 * (n_fs - 1)
     dma = pltpu.SemaphoreType.DMA
-    in_grad, grads, taps, rows_gu, rows_down = pl.pallas_call(
+    in_grad, down, gate, up, taps, rows_gate, rows_up, rows_down = pl.pallas_call(
         functools.partial(layer_kernel, n_rep, n_fs),
         out_shape=(
             jax.ShapeDtypeStruct((tok // 2, feat), bf16),
-            jax.ShapeDtypeStruct((pieces, LANES, cw), bf16),
-            jax.ShapeDtypeStruct((n_fs, chunks * 8, LANES), f32),
-            jax.ShapeDtypeStruct((2 * subs, LANES), f32),
-            jax.ShapeDtypeStruct((chunks * subs, LANES), f32),
+            jax.ShapeDtypeStruct((hid, feat), bf16),
+            jax.ShapeDtypeStruct((feat, hid), bf16),
+            jax.ShapeDtypeStruct((feat, hid), bf16),
+            jax.ShapeDtypeStruct((KW, hid), f32),
+            jax.ShapeDtypeStruct((1, feat), f32),
+            jax.ShapeDtypeStruct((1, feat), f32),
+            jax.ShapeDtypeStruct((1, hid), f32),
         ),
         in_specs=[vmem] * 6,
-        out_specs=(vmem, pl.BlockSpec(memory_space=pl.ANY), vmem, vmem, vmem),
+        out_specs=(vmem,) + (pl.BlockSpec(memory_space=pl.ANY),) * 3 + (vmem,) * 4,
         scratch_shapes=[
-            pltpu.VMEM((subs, LANES, tok), bf16),
-            pltpu.VMEM((chunks, 3, n_fs, tok, LANES), bf16),
-            pltpu.VMEM((chunks, 3, n_fs - 1, tok, LANES), bf16),
-            pltpu.VMEM((chunks, n_fs, LANES, tok), bf16),
+            pltpu.VMEM((subs, cw, tok), bf16),
+            pltpu.VMEM((chunks, 3, n_fs, tok // 2 + HALO, LANES), bf16),
+            pltpu.VMEM((chunks, 3, n_fs - 1, tok // 2 + HALO, LANES), bf16),
+            pltpu.VMEM((chunks, cw, tok), bf16),
             pltpu.VMEM((chunks, tok, cw), bf16),
             pltpu.VMEM((chunks, tok, cw), bf16),
-            pltpu.VMEM((pieces, LANES, cw), bf16),
-            pltpu.VMEM((pieces, LANES, cw), bf16),
-            pltpu.VMEM((pieces, LANES, cw), bf16),
-            pltpu.VMEM((pieces, LANES, cw), bf16),
+            pltpu.VMEM((pieces, cw, cw), bf16),
+            pltpu.VMEM((pieces, cw, cw), bf16),
+            pltpu.VMEM((pieces, cw, cw), bf16),
+            pltpu.VMEM((pieces, cw, cw), bf16),
             pltpu.VMEM((tok, feat), f32),
             pltpu.VMEM((tok, feat), bf16),
             pltpu.VMEM((tok // 2, feat), bf16),
-            pltpu.VMEM((n_fs, chunks * 8, LANES), f32),
-            pltpu.VMEM((n_fs, chunks * 8, LANES), f32),
-            pltpu.VMEM((n_fs, chunks * 8, LANES), f32),
-            pltpu.VMEM((pieces, LANES), f32),
-            pltpu.VMEM((pieces, LANES), f32),
-            pltpu.VMEM((n_fs - 1, pieces, LANES), f32),
-            dma((hops,)), dma((hops,)), dma((hops,)), dma((hops,)),
+            pltpu.VMEM((n_fs, chunks * KW, LANES), f32),
+            pltpu.VMEM((n_fs, chunks * KW, LANES), f32),
+            pltpu.VMEM((n_fs, chunks * KW, LANES), f32),
+            pltpu.VMEM((n_fs, chunks * KW, LANES), f32),
+            pltpu.VMEM((2 * pieces, LANES), f32),
+            pltpu.VMEM((2 * pieces, LANES), f32),
+            pltpu.VMEM((n_fs - 1, 2 * pieces, LANES), f32),
+            dma((hops,)), dma((hops,)), dma((chunks * 12,)), dma((chunks * 12,)),
             dma((pieces,)), dma((pieces,)), dma((pieces,)), dma((pieces,)), dma((pieces,)),
             dma((4 * (n_fs - 1) + 8,)),
         ],
@@ -507,14 +606,9 @@
             collective_id=0, has_side_effects=True, vmem_limit_bytes=60 * 1024 * 1024
         ),
     )(inputs, w_gate, w_up, conv_taps, w_down, out_grad)
-    grads = grads.reshape(chunks, 3, subs, LANES, cw)
-    grad_down = grads[:, 0].reshape(hid, feat).astype(f32)
-    grad_gate = grads[:, 1].transpose(1, 2, 0, 3).reshape(feat, hid).astype(f32)
-    grad_up = grads[:, 2].transpose(1, 2, 0, 3).reshape(feat, hid).astype(f32)
-    grad_taps = taps.reshape(n_fs, chunks, 8, LANES)[:, :, :KW].transpose(2, 1, 0, 3).reshape(KW, hid)
     return (
-        in_grad, grad_gate, grad_up, grad_down, grad_taps,
-        rows_gu[:subs].reshape(feat), rows_gu[subs:].reshape(feat), rows_down.reshape(hid),
+        in_grad, gate.astype(f32), up.astype(f32), down.astype(f32), taps,
+        rows_gate.reshape(feat), rows_up.reshape(feat), rows_down.reshape(hid),
     )
 
 

time: 194 us -> 184 us (0.948)
  local copies, waits for them, and re-layouts: 21.6 us -> 2.5 us
  Pallas kernels: 163 us -> 173 us
    unnamed x12 -> x18, local copies, waits for them, and re-layouts: 18.8 us -> 2.5 us
    pallas_call x1, Pallas kernels: 163 us -> 173 us  [fused_shards(): pl.pallas_call(functools.partial(layer_kernel, n_rep, n_fs), out_shape=(j...]
    slice x1 -> x0, other arithmetic: 6.02 us -> none  [fused_shards(): grad_down = grads[:, 0].reshape(hid, feat).astype(f32)]
    convert_element_type x1 -> x3, other arithmetic: 2.21 us -> 7.77 us  [the longest x1 3.6 us: fused_shards(): up.astype(f32)]
    reshape x2 -> x0, local copies, waits for them, and re-layouts: 1.97 us -> none  [the longest x1 1.35 us: fused_shards(): rows_gu[subs:].reshape(feat)]
where the time goes in v2:
time: 184 us
  Pallas kernels  173 us (94%)
  other arithmetic  8.39 us (5%)
  local copies, waits for them, and re-layouts  2.5 us (1%)
    pallas_call x1, Pallas kernels, fused_shards(): pl.pallas_call(functools.partial(layer_kernel, n_rep, n_fs), out_shape=(j...  173 us

profile of v2, /device:TPU:0, one launch (start us, length us, event | category | flops | bytes accessed | tf_op | source)
XLA Modules:
  0.0 184.2 jit_solution(14678939604080104169)
XLA Ops:
  0.6 172.6 %shard_map.125 = (bf16[256,512]{1,0:T(8,128)(2,1)}, bf16[1536,512]{1,0:T(8,128)(2,1)}, bf16[512,1536]{1,0:T(8,128)(2,1)}, bf16[512,1536]{1,0:T(8,128)(2,1)}, f32...) custom-call(bf16[512,512]{1,0:T(8,128)(2,1)} %x_ref.1, bf16[512,1536]{1,0:T(8,128)(2,1)} %wg_ref.1, ...), custom_call_target="tpu_custom_call" | custom-call | tf_op jit(solution)/shard_map/pallas_call | solution.py:566
  173.3 0.0 copy-start.1
  173.3 3.6 %convert_element_type.10 = f32[512,1536]{1,0:T(8,128)} convert(bf16[512,1536]{1,0:T(8,128)(2,1)} %get-tuple-element.18) | non-fusion elementwise | flops 786432 | bytes 4718592 | tf_op jit(solution)/shard_map/convert_element_type | solution.py:610
  176.9 0.0 copy-done.1
  176.9 0.0 copy-start
  176.9 2.1 %convert_element_type.11 = f32[1536,512]{1,0:T(8,128)} convert(bf16[1536,512]{1,0:T(8,128)(2,1)S(1)} %copy-done.1) | non-fusion elementwise | flops 786432 | bytes 4718592 | tf_op jit(solution)/shard_map/convert_element_type | solution.py:610
  179.0 0.0 copy-done
  179.0 0.0 copy-start.4
  179.0 0.0 copy-start.2
  179.0 0.0 copy-start.3
  179.0 0.0 copy-start.6
  179.0 0.0 copy-start.5
  179.0 2.1 %convert_element_type.9 = f32[512,1536]{1,0:T(8,128)} convert(bf16[512,1536]{1,0:T(8,128)(2,1)S(1)} %copy-done) | non-fusion elementwise | flops 786432 | bytes 4718592 | tf_op jit(solution)/shard_map/convert_element_type | solution.py:610
  181.1 0.0 copy-done.4
  181.1 0.6 reduce
  181.7 0.0 copy-done.2
  181.7 0.7 copy.18
  182.4 0.0 copy-done.3
  182.4 0.6 copy.19
  183.0 0.0 copy-done.6
  183.0 0.6 copy.20
  183.6 0.0 copy-done.5
  183.6 0.6 copy.21
Async XLA Ops:
  173.3 3.6 %copy-start.1 = (bf16[1536,512]{1,0:T(8,128)(2,1)S(1)}, bf16[1536,512]{1,0:T(8,128)(2,1)}, u32[]{:S(2)}) copy-start(bf16[1536,512]{1,0:T(8,128)(2,1)} %get-tuple-element.19) | copy-start | bytes 4718596
  176.9 2.1 %copy-start = (bf16[512,1536]{1,0:T(8,128)(2,1)S(1)}, bf16[512,1536]{1,0:T(8,128)(2,1)}, u32[]{:S(2)}) copy-start(bf16[512,1536]{1,0:T(8,128)(2,1)} %get-tuple-element.17) | copy-start | bytes 4718596
  179.0 2.1 %copy-start.4 = (f32[1,1536]{1,0:T(1,128)S(1)}, f32[1,1536]{1,0:T(1,128)}, u32[]{:S(2)}) copy-start(f32[1,1536]{1,0:T(1,128)} %get-tuple-element.23) | copy-start | bytes 18436
  179.0 2.7 %copy-start.2 = (bf16[256,512]{1,0:T(8,128)(2,1)S(1)}, bf16[256,512]{1,0:T(8,128)(2,1)}, u32[]{:S(2)}) copy-start(bf16[256,512]{1,0:T(8,128)(2,1)} %get-tuple-element.32) | copy-start | bytes 786436
  179.0 3.4 %copy-start.3 = (f32[3,1536]{1,0:T(4,128)S(1)}, f32[3,1536]{1,0:T(4,128)}, u32[]{:S(2)}) copy-start(f32[3,1536]{1,0:T(4,128)} %get-tuple-element.36) | copy-start | bytes 55300
  179.0 4.0 %copy-start.6 = (f32[1,512]{1,0:T(1,128)S(1)}, f32[1,512]{1,0:T(1,128)}, u32[]{:S(2)}) copy-start(f32[1,512]{1,0:T(1,128)} %get-tuple-element.21) | copy-start | bytes 6148
  179.0 4.6 %copy-start.5 = (f32[1,512]{1,0:T(1,128)S(1)}, f32[1,512]{1,0:T(1,128)}, u32[]{:S(2)}) copy-start(f32[1,512]{1,0:T(1,128)} %get-tuple-element.22) | copy-start | bytes 6148

commit v3 on v2

--- a/solution.py
+++ b/solution.py
@@ -97,7 +97,7 @@
 CW = 256
 HALO = 16
 MID_LAG = 3
-OUT_LAG = 8
+OUT_LAG = 18
 MESH_ID = pl.DeviceIdType.MESH
 
 
@@ -417,19 +417,19 @@
 
     forward(0, 0)
     for c in range(chunks):
-        segment(c, 0)
         if c > 0:
             advance(c + 1)
-        forward(c, 1)
-        if c > 0:
-            forward(c, 2)
+        segment(c, 0)
+        if c == 0:
+            forward(c, 1)
         segment(c, 1)
         if c == 0:
             forward(c, 2)
             advance(c + 1)
         segment(c, 2)
         if c + 1 < chunks:
-            forward(c + 1, 0)
+            for tensor in range(3):
+                forward(c + 1, tensor)
         input_term(c)
 
     m = 2 * (n_fs - 1)

time: 184 us -> 174 us (0.946)
  Pallas kernels: 173 us -> 162 us
    pallas_call x1, Pallas kernels: 173 us -> 162 us  [fused_shards(): pl.pallas_call(functools.partial(layer_kernel, n_rep, n_fs), out_shape=(j...]
where the time goes in v3:
time: 174 us
  Pallas kernels  162 us (93%)
  other arithmetic  8.39 us (5%)
  local copies, waits for them, and re-layouts  2.5 us (1%)
    pallas_call x1, Pallas kernels, fused_shards(): pl.pallas_call(functools.partial(layer_kernel, n_rep, n_fs), out_shape=(j...  162 us
    convert_element_type x1, other arithmetic, fused_shards(): up.astype(f32)  3.6 us

profile of v3, /device:TPU:0, one launch (start us, length us, event | category | flops | bytes accessed | tf_op | source)
XLA Modules:
  0.0 173.9 jit_solution(516012700803833928)
XLA Ops:
  0.6 162.3 %shard_map.125 = (bf16[256,512]{1,0:T(8,128)(2,1)}, bf16[1536,512]{1,0:T(8,128)(2,1)}, bf16[512,1536]{1,0:T(8,128)(2,1)}, bf16[512,1536]{1,0:T(8,128)(2,1)}, f32...) custom-call(bf16[512,512]{1,0:T(8,128)(2,1)} %x_ref.1, bf16[512,1536]{1,0:T(8,128)(2,1)} %wg_ref.1, ...), custom_call_target="tpu_custom_call" | custom-call | tf_op jit(solution)/shard_map/pallas_call | solution.py:566
  163.0 0.0 copy-start.1
  163.0 3.6 %convert_element_type.10 = f32[512,1536]{1,0:T(8,128)} convert(bf16[512,1536]{1,0:T(8,128)(2,1)} %get-tuple-element.18) | non-fusion elementwise | flops 786432 | bytes 4718592 | tf_op jit(solution)/shard_map/convert_element_type | solution.py:610
  166.6 0.0 copy-done.1
  166.6 0.0 copy-start
  166.6 2.1 %convert_element_type.11 = f32[1536,512]{1,0:T(8,128)} convert(bf16[1536,512]{1,0:T(8,128)(2,1)S(1)} %copy-done.1) | non-fusion elementwise | flops 786432 | bytes 4718592 | tf_op jit(solution)/shard_map/convert_element_type | solution.py:610
  168.7 0.0 copy-done
  168.7 0.0 copy-start.4
  168.7 0.0 copy-start.2
  168.7 0.0 copy-start.3
  168.7 0.0 copy-start.6
  168.7 0.0 copy-start.5
  168.7 2.1 %convert_element_type.9 = f32[512,1536]{1,0:T(8,128)} convert(bf16[512,1536]{1,0:T(8,128)(2,1)S(1)} %copy-done) | non-fusion elementwise | flops 786432 | bytes 4718592 | tf_op jit(solution)/shard_map/convert_element_type | solution.py:610
  170.8 0.0 copy-done.4
  170.8 0.6 reduce
  171.4 0.0 copy-done.2
  171.4 0.7 copy.18
  172.1 0.0 copy-done.3
  172.1 0.6 copy.19
  172.7 0.0 copy-done.6
  172.7 0.6 copy.20
  173.3 0.0 copy-done.5
  173.3 0.6 copy.21
Async XLA Ops:
  163.0 3.6 %copy-start.1 = (bf16[1536,512]{1,0:T(8,128)(2,1)S(1)}, bf16[1536,512]{1,0:T(8,128)(2,1)}, u32[]{:S(2)}) copy-start(bf16[1536,512]{1,0:T(8,128)(2,1)} %get-tuple-element.19) | copy-start | bytes 4718596
  166.6 2.1 %copy-start = (bf16[512,1536]{1,0:T(8,128)(2,1)S(1)}, bf16[512,1536]{1,0:T(8,128)(2,1)}, u32[]{:S(2)}) copy-start(bf16[512,1536]{1,0:T(8,128)(2,1)} %get-tuple-element.17) | copy-start | bytes 4718596
  168.7 2.1 %copy-start.4 = (f32[1,1536]{1,0:T(1,128)S(1)}, f32[1,1536]{1,0:T(1,128)}, u32[]{:S(2)}) copy-start(f32[1,1536]{1,0:T(1,128)} %get-tuple-element.23) | copy-start | bytes 18436
  168.7 2.7 %copy-start.2 = (bf16[256,512]{1,0:T(8,128)(2,1)S(1)}, bf16[256,512]{1,0:T(8,128)(2,1)}, u32[]{:S(2)}) copy-start(bf16[256,512]{1,0:T(8,128)(2,1)} %get-tuple-element.32) | copy-start | bytes 786436
  168.7 3.4 %copy-start.3 = (f32[3,1536]{1,0:T(4,128)S(1)}, f32[3,1536]{1,0:T(4,128)}, u32[]{:S(2)}) copy-start(f32[3,1536]{1,0:T(4,128)} %get-tuple-element.36) | copy-start | bytes 55300
  168.7 4.0 %copy-start.6 = (f32[1,512]{1,0:T(1,128)S(1)}, f32[1,512]{1,0:T(1,128)}, u32[]{:S(2)}) copy-start(f32[1,512]{1,0:T(1,128)} %get-tuple-element.21) | copy-start | bytes 6148
  168.7 4.6 %copy-start.5 = (f32[1,512]{1,0:T(1,128)S(1)}, f32[1,512]{1,0:T(1,128)}, u32[]{:S(2)}) copy-start(f32[1,512]{1,0:T(1,128)} %get-tuple-element.22) | copy-start | bytes 6148
